TPU v7x, 32 devices: a whole 2x2x4 slice. The times are simulated.
32 devices in a mesh: sp: 8 (over z, x), dp: 4 (over y, core).
Axes of the slice: x: 2, y: 2, z: 4, core: 2. Of those that a mesh axis runs over, the one named last changes fastest.
Arguments:
- tokens: bfloat16 [4, 3072, 2048], P('dp', 'sp'), may hold values from -6 to 6
- q_weight: bfloat16 [2048, 1024], P(('sp', 'dp')), may hold values from -0.13258252 to 0.13258252
- k_weight: bfloat16 [2048, 256], P(('sp', 'dp')), may hold values from -0.13258252 to 0.13258252
- v_weight: bfloat16 [2048, 256], P(('sp', 'dp')), may hold values from -0.125 to 0.125
- out_weight: bfloat16 [1024, 2048], P(None, ('sp', 'dp')), may hold values from -6 to 6
- q_gain: float32 [64], replicated, may hold values from 0.5 to 8
- k_gain: float32 [64], replicated, may hold values from 0.5 to 8
Outputs:
- mixed: bfloat16 [4, 3072, 2048], P('dp', 'sp')
All inputs are finite; a program needn't handle non-finite values.
Results may differ from a plain program's by a relative error of at most 0.0055.
The roundings to bfloat16 on the way count: a program that leaves them out, or rounds other values in their place, can miss the bound.
Values may be sent and summed in bfloat16 or wider, within the bound.
A program may use at most 128 MiB of HBM per device.

v0:
```python
import math

import jax
import jax.numpy as jnp
from jax import lax
from jax.sharding import PartitionSpec as P

GRID_W = 64


epsilon = 1e-06
rope_base = 10000.0


def normalize(tensor, gain_vec):
    mean_sq = jnp.mean(tensor * tensor, axis=-1, keepdims=True)
    return tensor * lax.rsqrt(mean_sq + epsilon) * gain_vec


def rotate(tensor, offset):
    row_count = tensor.shape[0]
    head_width = tensor.shape[2]
    quarter = head_width // 4
    half_width = head_width // 2
    positions = jnp.arange(row_count, dtype=jnp.int32) + offset
    frequency = rope_base ** (-jnp.arange(quarter, dtype=jnp.float32) / quarter)

    def rotate_pair(segment, coords):
        angles = coords.astype(jnp.float32)[:, None] * frequency[None, :]
        cosine = jnp.cos(angles)[:, None, :]
        sine_val = jnp.sin(angles)[:, None, :]
        low_half = segment[..., :quarter]
        high_half = segment[..., quarter:]
        return jnp.concatenate(
            [low_half * cosine - high_half * sine_val, high_half * cosine + low_half * sine_val],
            axis=-1,
        )

    return jnp.concatenate(
        [
            rotate_pair(tensor[..., :half_width], positions // GRID_W),
            rotate_pair(tensor[..., half_width:], positions % GRID_W),
        ],
        axis=-1,
    )


def attend(query_rows, key_rows, value_rows):
    row_count, head_width = query_rows.shape
    block_rows = math.gcd(row_count, 512)
    score_scale = head_width ** (-0.5)

    def attend_block(segment):
        scores = (
            lax.dot_general(
                segment, key_rows, (((1,), (1,)), ((), ())), preferred_element_type=jnp.float32
            )
            * score_scale
        )
        row_max = jnp.max(scores, axis=-1, keepdims=True)
        weights = jnp.exp(scores - row_max)
        shares = (weights / jnp.sum(weights, axis=-1, keepdims=True)).astype(jnp.bfloat16)
        return jnp.dot(shares, value_rows, preferred_element_type=jnp.float32).astype(jnp.bfloat16)

    blocks = query_rows.reshape(row_count // block_rows, block_rows, head_width)
    return lax.map(attend_block, blocks).reshape(row_count, head_width)


def per_device(tokens, q_weight, k_weight, v_weight, out_weight, q_gain, k_gain):
    rows_in = tokens[0]
    tok_count = rows_in.shape[0]
    head_width = q_gain.shape[0]
    q_width = out_weight.shape[0]
    kv_width = k_weight.shape[1]
    q_heads = q_width // head_width
    kv_heads = kv_width // head_width
    group_size = q_heads // kv_heads
    sp_count = lax.axis_size("sp")
    offset = lax.axis_index("sp") * tok_count
    weight_rows = (
        lax.all_gather(q_weight, ("sp", "dp"), axis=0, tiled=True),
        lax.all_gather(k_weight, ("sp", "dp"), axis=0, tiled=True),
        lax.all_gather(v_weight, ("sp", "dp"), axis=0, tiled=True),
    )
    query_raw, key_raw, value_raw = tuple(
        (
            jnp.dot(rows_in, rows_part, preferred_element_type=jnp.float32)
            for rows_part in weight_rows
        )
    )
    queries = rotate(
        normalize(query_raw.reshape(tok_count, q_heads, head_width), q_gain), offset
    ).astype(jnp.bfloat16)
    keys_rot = rotate(
        normalize(key_raw.reshape(tok_count, kv_heads, head_width), k_gain), offset
    ).astype(jnp.bfloat16)
    values_dev = value_raw.astype(jnp.bfloat16)
    keys_wide = jnp.broadcast_to(
        keys_rot[:, :, None, :], (tok_count, kv_heads, group_size, head_width)
    ).reshape(tok_count, q_width)
    values_wide = jnp.broadcast_to(
        values_dev.reshape(tok_count, kv_heads, 1, head_width),
        (tok_count, kv_heads, group_size, head_width),
    ).reshape(tok_count, q_width)
    q_local, k_local, v_local = (
        lax.all_to_all(
            queries.reshape(tok_count, q_width), "sp", split_axis=1, concat_axis=0, tiled=True
        ),
        lax.all_to_all(keys_wide, "sp", split_axis=1, concat_axis=0, tiled=True),
        lax.all_to_all(values_wide, "sp", split_axis=1, concat_axis=0, tiled=True),
    )
    local_heads = q_width // sp_count // head_width
    outputs = []
    for head_index in range(local_heads):
        low_col = head_index * head_width
        outputs.append(
            attend(
                q_local[:, low_col : low_col + head_width],
                k_local[:, low_col : low_col + head_width],
                v_local[:, low_col : low_col + head_width],
            )
        )
    head_results = jnp.concatenate(outputs, axis=1)
    attended = lax.all_to_all(head_results, "sp", split_axis=0, concat_axis=1, tiled=True)
    result = jnp.dot(
        attended,
        lax.all_gather(out_weight, ("sp", "dp"), axis=1, tiled=True),
        preferred_element_type=jnp.float32,
    ).astype(jnp.bfloat16)
    return result[None]


def solution(mesh):
    return jax.shard_map(
        per_device,
        mesh=mesh,
        in_specs=(
            P("dp", "sp", None),
            P(("sp", "dp"), None),
            P(("sp", "dp"), None),
            P(("sp", "dp"), None),
            P(None, ("sp", "dp")),
            P(),
            P(),
        ),
        out_specs=P("dp", "sp", None),
        check_vma=False,
    )
```

profile of v0, /device:TPU:0, one launch (start us, length us, event | category | flops | bytes accessed | tf_op | source)
XLA Modules:
  0.0 334.7 jit_solution(1105141185171821577)
XLA Ops:
  9.0 57.6 %all-gather.7.cloned.1.call-done = bf16[2048,256]{1,0:T(8,128)(2,1)} async-done(((bf16[64,256]{1,0:T(8,128)(2,1)}), bf16[2048,256]{1,0:T(8,128)(2,1)}) %all-gather.7.cloned.1.call-update) | async-done | bytes 1048592 | tf_op jit(solution)/shard_map/all_gather | solution.py:82
  70.1 4.3 %all-to-all-start.1 = ((bf16[384,8,128]{0,2,1:T(8,128)(2,1)}), bf16[384,8,128]{0,2,1:T(8,128)(2,1)S(1)}, u32[]{:S(2)}, u32[]{:S(2)}) async-start(bf16[384,8,128]{0,2,1:T(8,128)(2,1)} %bitcast.14), calls=%async_computation.1 | async-start | bytes 1572864 | tf_op jit(solution)/shard_map/all_to_all | solution.py:109
  74.4 51.6 %all-gather.9.cloned.1.call-done = bf16[2048,256]{1,0:T(8,128)(2,1)} async-done(((bf16[64,256]{1,0:T(8,128)(2,1)}), bf16[2048,256]{1,0:T(8,128)(2,1)}) %all-gather.9.cloned.1.call-update) | async-done | bytes 1048592 | tf_op jit(solution)/shard_map/all_gather | solution.py:83
  126.0 2.0 fusion.27
  129.0 4.3 %all-to-all-start.2 = ((bf16[384,8,128]{0,2,1:T(8,128)(2,1)}), bf16[384,8,128]{0,2,1:T(8,128)(2,1)S(1)}, u32[]{:S(2)}, u32[]{:S(2)}) async-start(bf16[384,8,128]{0,2,1:T(8,128)(2,1)} %bitcast.90), calls=%async_computation.2 | async-start | bytes 1572864 | tf_op jit(solution)/shard_map/all_to_all | solution.py:110
  135.1 21.5 %all-to-all-done.2 = bf16[384,8,128]{0,2,1:T(8,128)(2,1)S(1)} async-done(((bf16[384,8,128]{0,2,1:T(8,128)(2,1)}), bf16[384,8,128]{0,2,1:T(8,128)(2,1)S(1)}, u32[]{:S(2)}, u32[]{:S(2)}) %all-to-all-start.2) | async-done | bytes 786464 | tf_op jit(solution)/shard_map/all_to_all | solution.py:110
  157.8 35.9 %all-gather.5.cloned.1.call-done = bf16[2048,1024]{1,0:T(8,128)(2,1)} async-done(((bf16[64,1024]{1,0:T(8,128)(2,1)}), bf16[2048,1024]{1,0:T(8,128)(2,1)}) %all-gather.5.cloned.1.call-update) | async-done | bytes 4194320 | tf_op jit(solution)/shard_map/all_gather | solution.py:81
  193.8 6.5 %copy.26 = bf16[1024,2048]{1,0:T(8,128)(2,1)} copy(bf16[1024,2048]{0,1:T(8,128)(2,1)} %bitcast.85) | data formatting | bytes 8388608 | tf_op jit(solution)/shard_map/dot_general | solution.py:87
  200.3 4.6 %multiply_reduce_fusion.2 = (f32[384,16]{0,1:T(8,128)S(1)}, f32[384,16,64]{0,2,1:T(8,128)S(1)}) fusion(bf16[16,64,2048]{2,1,0:T(8,128)(2,1)} %bitcast.86, bf16[1,384,2048]{2,1,0:T(8,128)(2,1)S(1)} %copy-done), kind=kOutput, calls=%fused_computation.35 | convolution fusion | flops 1611393024 | bytes 7364608 | tf_op jit(solution)/shard_map/dot_general | solution.py:87
  206.7 4.4 %all-to-all-start = ((bf16[384,8,128]{2,0,1:T(8,128)(2,1)}), bf16[384,8,128]{2,0,1:T(8,128)(2,1)}, u32[]{:S(2)}, u32[]{:S(2)}) async-start(bf16[384,8,128]{2,0,1:T(8,128)(2,1)} %copy.27), calls=%async_computation | async-start | bytes 1572864 | tf_op jit(solution)/shard_map/all_to_all | solution.py:106
  211.2 1.7 fusion.36
  212.9 2.8 fusion.35
  215.7 20.6 %all-to-all-done = bf16[384,8,128]{2,0,1:T(8,128)(2,1)} async-done(((bf16[384,8,128]{2,0,1:T(8,128)(2,1)}), bf16[384,8,128]{2,0,1:T(8,128)(2,1)}, u32[]{:S(2)}, u32[]{:S(2)}) %all-to-all-start) | async-done | bytes 786464 | tf_op jit(solution)/shard_map/all_to_all | solution.py:106
  236.3 2.9 fusion.37
  239.2 28.8 %while.20 = (s32[]{:T(128)}, bf16[6,512,64]{1,2,0:T(8,128)(2,1)S(1)}, bf16[6,512,64]{2,1,0:T(8,128)(2,1)}, bf16[3072,64]{1,0:T(8,128)(2,1)S(1)}, bf16[3072,64]{1,0:T(8,128)(2,1)}, /*index=5*/s32[]{:T(128)}) while((s32[]{:T(128)}, bf16[6,512,64]{1,2,0:T(8,128)(2,1)S(1)}, bf16[6,512,64]{2,1,0:T(8,128)(2,1)}, bf16[3072,64]{1,0:T(8,128)(2,1)S(1)}, ...), condition=%wide.region_5.6_spmd, body=%wide.region_2.5_spmd.sunk | while | flops 416840704 | bytes 21834340 | solution.py:66
  239.3 2.0 multiply_reduce_fusion.6
  244.0 2.0 multiply_reduce_fusion.6
  248.9 2.0 multiply_reduce_fusion.6
  253.7 2.0 multiply_reduce_fusion.6
  258.5 2.0 multiply_reduce_fusion.6
  263.3 2.0 multiply_reduce_fusion.6
  268.6 28.7 %while.21 = (s32[]{:T(128)}, bf16[6,512,64]{1,2,0:T(8,128)(2,1)S(1)}, bf16[6,512,64]{2,1,0:T(8,128)(2,1)}, bf16[3072,64]{1,0:T(8,128)(2,1)S(1)}, bf16[3072,64]{1,0:T(8,128)(2,1)}, /*index=5*/s32[]{:T(128)}) while((s32[]{:T(128)}, bf16[6,512,64]{1,2,0:T(8,128)(2,1)S(1)}, bf16[6,512,64]{2,1,0:T(8,128)(2,1)}, bf16[3072,64]{1,0:T(8,128)(2,1)S(1)}, ...), condition=%wide.region_9.10_spmd, body=%wide.region_6.9_spmd.sunk | while | flops 416840704 | bytes 21834340 | solution.py:66
  268.6 2.0 multiply_reduce_fusion.7
  273.4 2.0 multiply_reduce_fusion.7
  278.2 2.0 multiply_reduce_fusion.7
  281.3 1.6 fusion.62
  283.0 2.0 multiply_reduce_fusion.7
  287.8 2.0 multiply_reduce_fusion.7
  292.6 2.0 multiply_reduce_fusion.7
  298.9 3.7 %all-to-all-start.3 = ((bf16[8,384,128]{1,2,0:T(8,128)(2,1)}), bf16[8,384,128]{1,2,0:T(8,128)(2,1)S(1)}, u32[]{:S(2)}, u32[]{:S(2)}) async-start(bf16[8,384,128]{1,2,0:T(8,128)(2,1)} %copy.33), calls=%async_computation.3 | async-start | bytes 1572864 | tf_op jit(solution)/shard_map/all_to_all | solution.py:124
  302.6 20.4 %all-to-all-done.3 = bf16[8,384,128]{1,2,0:T(8,128)(2,1)S(1)} async-done(((bf16[8,384,128]{1,2,0:T(8,128)(2,1)}), bf16[8,384,128]{1,2,0:T(8,128)(2,1)S(1)}, u32[]{:S(2)}, u32[]{:S(2)}) %all-to-all-start.3) | async-done | bytes 786464 | tf_op jit(solution)/shard_map/all_to_all | solution.py:124
  323.0 5.2 %fusion.20 = bf16[1,384,2048]{2,1,0:T(8,128)(2,1)} fusion(bf16[384,1024]{0,1:T(8,128)(2,1)S(1)} %bitcast.95, bf16[1024,2048]{0,1:T(8,128)(2,1)} %all-gather.11.cloned.1.call-done), kind=kOutput, calls=%fused_computation.27 | convolution fusion | flops 1611399168 | bytes 6553600 | tf_op jit(solution)/shard_map/dot_general | solution.py:125
  (89 shorter events, 45.6 us)
Async XLA Ops:
  6.5 61.6 %copy-start = (bf16[1,384,2048]{2,1,0:T(8,128)(2,1)S(1)}, bf16[1,384,2048]{2,1,0:T(8,128)(2,1)}, u32[]{:S(2)}) copy-start(bf16[1,384,2048]{2,1,0:T(8,128)(2,1)} %param.11) | copy-start | bytes 4718596
  6.5 62.4 %copy-start.3 = (f32[64]{0:T(128)S(1)}, f32[64]{0:T(128)}, u32[]{:S(2)}) copy-start(f32[64]{0:T(128)} %param.17) | copy-start | bytes 772
  6.5 60.1 %all-gather.7.cloned.1.call-start = ((), (), s32[]{:S(2)}) async-start(), calls=%async_computation.5 | async-start | bytes 1081344 | tf_op jit(solution)/shard_map/all_gather | solution.py:82
  7.3 118.8 %all-gather.9.cloned.1.call-start = ((), (), s32[]{:S(2)}) async-start(), calls=%async_computation.6 | async-start | bytes 1081344 | tf_op jit(solution)/shard_map/all_gather | solution.py:83
  8.0 185.8 %all-gather.5.cloned.1.call-start = ((), (), s32[]{:S(2)}) async-start(), calls=%async_computation.4 | async-start | bytes 4325376 | tf_op jit(solution)/shard_map/all_gather | solution.py:81
  70.1 57.9 %all-to-all-start.1 = ((bf16[384,8,128]{0,2,1:T(8,128)(2,1)}), bf16[384,8,128]{0,2,1:T(8,128)(2,1)S(1)}, u32[]{:S(2)}, u32[]{:S(2)}) async-start(bf16[384,8,128]{0,2,1:T(8,128)(2,1)} %bitcast.14), calls=%async_computation.1 | async-start | bytes 1572864 | tf_op jit(solution)/shard_map/all_to_all | solution.py:109
  129.0 27.6 %all-to-all-start.2 = ((bf16[384,8,128]{0,2,1:T(8,128)(2,1)}), bf16[384,8,128]{0,2,1:T(8,128)(2,1)S(1)}, u32[]{:S(2)}, u32[]{:S(2)}) async-start(bf16[384,8,128]{0,2,1:T(8,128)(2,1)} %bitcast.90), calls=%async_computation.2 | async-start | bytes 1572864 | tf_op jit(solution)/shard_map/all_to_all | solution.py:110
  133.3 169.3 %all-gather.11.cloned.1.call-start = ((), (), s32[]{:S(2)}) async-start(), calls=%async_computation.7 | async-start | bytes 4325376 | tf_op jit(solution)/shard_map/all_gather | solution.py:127
  200.3 4.6 %copy-start.4 = (f32[64]{0:T(128)S(1)}, f32[64]{0:T(128)}, u32[]{:S(2)}) copy-start(f32[64]{0:T(128)} %param.16) | copy-start | bytes 772
  206.7 29.6 %all-to-all-start = ((bf16[384,8,128]{2,0,1:T(8,128)(2,1)}), bf16[384,8,128]{2,0,1:T(8,128)(2,1)}, u32[]{:S(2)}, u32[]{:S(2)}) async-start(bf16[384,8,128]{2,0,1:T(8,128)(2,1)} %copy.27), calls=%async_computation | async-start | bytes 1572864 | tf_op jit(solution)/shard_map/all_to_all | solution.py:106
  241.2 1.2 copy-start.2
  246.1 1.2 copy-start.2
  250.9 1.2 copy-start.2
  255.7 1.2 copy-start.2
  260.4 1.2 copy-start.2
  265.3 1.2 copy-start.2
  270.6 1.2 copy-start.1
  275.4 1.2 copy-start.1
  280.2 1.2 copy-start.1
  285.0 1.2 copy-start.1
  289.8 1.2 copy-start.1
  294.5 1.2 copy-start.1
  298.9 24.1 %all-to-all-start.3 = ((bf16[8,384,128]{1,2,0:T(8,128)(2,1)}), bf16[8,384,128]{1,2,0:T(8,128)(2,1)S(1)}, u32[]{:S(2)}, u32[]{:S(2)}) async-start(bf16[8,384,128]{1,2,0:T(8,128)(2,1)} %copy.33), calls=%async_computation.3 | async-start | bytes 1572864 | tf_op jit(solution)/shard_map/all_to_all | solution.py:124
Sparse Core Ops, SparseCore 0:
  10.2 56.3 all-gather.6
  69.5 56.4 all-gather.8
  128.9 64.7 all-gather.4
  196.5 66.2 all-gather.10
where the time goes:
time: 336 us; the launch traced here: 335 us
  waiting for transfers between devices  210 us (62%)
  matrix products  55.7 us (17%)
  local copies, waits for them, and re-layouts  23 us (7%)
  starting transfers between devices  16.8 us (5%)
  other arithmetic  15.1 us (4%)
  between operations  13.3 us (4%)
    all_gather x1, waiting for transfers between devices, per_device(): lax.all_gather(k_weight, ('sp', 'dp'), axis=0, tiled=True)  57.6 us
    all_gather x1, waiting for transfers between devices, per_device(): lax.all_gather(v_weight, ('sp', 'dp'), axis=0, tiled=True)  51.6 us
    all_gather x1, waiting for transfers between devices, per_device(): lax.all_gather(q_weight, ('sp', 'dp'), axis=0, tiled=True)  35.9 us
    dot_general x12, matrix products, attend_block(): lax.dot_general(segment, key_rows, (((1,), (1,)), ((), ())), preferred_el...  23.7 us
    all_to_all x1, waiting for transfers between devices, per_device(): lax.all_to_all(values_wide, 'sp', split_axis=1, concat_axis=0, tiled=True)  21.5 us
    all_to_all x1, waiting for transfers between devices, per_device(): lax.all_to_all(queries.reshape(tok_count, q_width), 'sp', split_axis=1, c...  20.6 us
    all_to_all x1, waiting for transfers between devices, per_device(): lax.all_to_all(head_results, 'sp', split_axis=0, concat_axis=1, tiled=True)  20.4 us
    dot_general x12, matrix products, attend_block(): jnp.dot(shares, value_rows, preferred_element_type=jnp.float32)  19.5 us
  transfers between devices with their start and end apart: 8, of which 6 were waited for; matrix products, arithmetic and copies ran while one was open for 26% of the time, Pallas kernels for 0%

commit v1 on v0

--- a/solution.py
+++ b/solution.py
@@ -1,15 +1,472 @@
+import functools
 import math
 
 import jax
 import jax.numpy as jnp
 from jax import lax
+from jax.experimental import pallas as pl
+from jax.experimental.pallas import tpu as pltpu
 from jax.sharding import PartitionSpec as P
 
 GRID_W = 64
-
-
+CORES = 2
 epsilon = 1e-06
 rope_base = 10000.0
+VMEM_BYTES = 60 * 1024 * 1024
+
+
+def tables(tok_count, head_width, offset, width):
+    quarter = head_width // 4
+    positions = jnp.arange(tok_count, dtype=jnp.int32) + offset
+    frequency = rope_base ** (-jnp.arange(quarter, dtype=jnp.float32) / quarter)
+    row_angle = (positions // GRID_W).astype(jnp.float32)[:, None] * frequency[None, :]
+    col_angle = (positions % GRID_W).astype(jnp.float32)[:, None] * frequency[None, :]
+    cos = jnp.concatenate([jnp.cos(row_angle)] * 2 + [jnp.cos(col_angle)] * 2, axis=1)
+    sin_r, sin_c = jnp.sin(row_angle), jnp.sin(col_angle)
+    sin = jnp.concatenate([-sin_r, sin_r, -sin_c, sin_c], axis=1)
+    return jnp.tile(cos, (1, width // head_width)), jnp.tile(sin, (1, width // head_width))
+
+
+class Net:
+    def __init__(self, dims):
+        self.zs, self.xs, self.ys = dims
+        sp, dp = lax.axis_index("sp"), lax.axis_index("dp")
+        self.z, self.x = sp // self.xs, sp % self.xs
+        self.y, self.c = dp // CORES, dp % CORES
+        self.ox, self.oy, self.oc = 1 - self.x, 1 - self.y, 1 - self.c
+
+    def at(self, z=None, x=None, y=None, c=None):
+        z = self.z if z is None else z
+        x = self.x if x is None else x
+        y = self.y if y is None else y
+        c = self.c if c is None else c
+        return {"sp": z * self.xs + x, "dp": y * CORES + c}
+
+    def sides(self):
+        return ((-1, 1), (1, -1))
+
+    def inside(self, z):
+        return jnp.logical_and(z >= 0, z < self.zs)
+
+
+def greet(net, fixed):
+    barrier = pltpu.get_barrier_semaphore()
+    for where in fixed:
+        pl.semaphore_signal(barrier, inc=1, device_id=where, device_id_type=pl.DeviceIdType.MESH)
+    for step in (-1, 1):
+
+        @pl.when(net.inside(net.z + step))
+        def _():
+            pl.semaphore_signal(
+                barrier,
+                inc=1,
+                device_id=net.at(z=net.z + step),
+                device_id_type=pl.DeviceIdType.MESH,
+            )
+
+    along = jnp.minimum(net.z, 1) + jnp.minimum(net.zs - 1 - net.z, 1)
+    pl.semaphore_wait(barrier, len(fixed) + along)
+
+
+def remote(src, dst, send, recv, where):
+    return pltpu.make_async_remote_copy(
+        src_ref=src,
+        dst_ref=dst,
+        send_sem=send,
+        recv_sem=recv,
+        device_id=where,
+        device_id_type=pl.DeviceIdType.MESH,
+    )
+
+
+def gather_weights(net, w_own, wbuf, own_sem, zs_sem, zr_sem, xs, xr, ys, yr, ds, dr, cs, cr):
+    half = wbuf.shape[-1] // 2
+    halves = (pl.ds(0, half), pl.ds(half, half))
+
+    def block(z, x, y, c):
+        return wbuf.at[z, x, y, c]
+
+    def part(z, x, y, c, h):
+        return wbuf.at[z, x, y, c, :, halves[h]]
+
+    def to_x(k, z, src=None):
+        dst = block(z, net.x, net.y, net.c)
+        return remote(dst if src is None else src, dst, xs.at[k], xr.at[k], net.at(x=net.ox))
+
+    def from_x(k, z):
+        b = block(z, net.ox, net.y, net.c)
+        return remote(b, b, xs.at[k], xr.at[k], net.at(x=net.ox))
+
+    def to_y(k, z, src=None):
+        dst = block(z, net.x, net.y, net.c)
+        return remote(dst if src is None else src, dst, ys.at[k], yr.at[k], net.at(y=net.oy))
+
+    def from_y(k, z):
+        b = block(z, net.x, net.oy, net.c)
+        return remote(b, b, ys.at[k], yr.at[k], net.at(y=net.oy))
+
+    def diag_to(k, z, h):
+        if h == 0:
+            b = part(z, net.ox, net.y, net.c, 0)
+            return remote(b, b, ds.at[0, k], dr.at[0, k], net.at(y=net.oy))
+        b = part(z, net.x, net.oy, net.c, 1)
+        return remote(b, b, ds.at[1, k], dr.at[1, k], net.at(x=net.ox))
+
+    def diag_from(k, z, h):
+        b = part(z, net.ox, net.oy, net.c, h)
+        where = net.at(y=net.oy) if h == 0 else net.at(x=net.ox)
+        return remote(b, b, ds.at[h, k], dr.at[h, k], where)
+
+    def core(kind, k, z, c, src=None):
+        x = net.ox if kind in (1, 3, 4) else net.x
+        y = net.oy if kind in (2, 3, 4) else net.y
+        b = part(z, x, y, c, kind - 3) if kind >= 3 else block(z, x, y, c)
+        return remote(
+            b if src is None else src, b, cs.at[kind, k], cr.at[kind, k], net.at(c=net.oc)
+        )
+
+    def to_z(k, z, step, src=None):
+        dst = block(z, net.x, net.y, net.c)
+        return remote(
+            dst if src is None else src, dst, zs_sem.at[k], zr_sem.at[k], net.at(z=net.z + step)
+        )
+
+    def slots():
+        for step in range(net.zs - 1):
+            for side in range(2):
+                sign = -1 if side == 0 else 1
+                yield step, side, 1 + 2 * step + side, net.z + sign * (step + 1), -sign
+
+    def spread(k, z, src=None):
+        to_x(k, z, src).start()
+        to_y(k, z, src).start()
+        core(0, k, z, net.c, src).start()
+
+    def second(k, z):
+        from_x(k, z).wait_recv()
+        diag_to(k, z, 0).start()
+        core(1, k, z, net.c).start()
+        from_y(k, z).wait_recv()
+        diag_to(k, z, 1).start()
+        core(2, k, z, net.c).start()
+
+    def third(k, z):
+        diag_from(k, z, 0).wait_recv()
+        core(3, k, z, net.c).start()
+        diag_from(k, z, 1).wait_recv()
+        core(4, k, z, net.c).start()
+
+    mine = pltpu.make_async_copy(w_own, block(net.z, net.x, net.y, net.c), own_sem)
+    mine.start()
+    for side, step in ((0, 1), (1, -1)):
+
+        @pl.when(net.inside(net.z + step))
+        def _():
+            to_z(1 + side, net.z, step, w_own).start()
+
+    spread(0, net.z, w_own)
+    stages = [[(0, net.z)]]
+    for s in range(net.zs - 1):
+        here = []
+        for step, side, k, z, onward in slots():
+            if step != s:
+                continue
+
+            @pl.when(net.inside(z))
+            def _():
+                to_z(k, z, 0).wait_recv()
+                if s < net.zs - 2:
+
+                    @pl.when(net.inside(net.z + onward))
+                    def _():
+                        to_z(k + 2, z, onward).start()
+
+                spread(k, z)
+
+            here.append((k, z))
+        for k, z in stages[-1]:
+
+            @pl.when(net.inside(z))
+            def _():
+                second(k, z)
+
+        if len(stages) > 1:
+            for k, z in stages[-2]:
+
+                @pl.when(net.inside(z))
+                def _():
+                    third(k, z)
+
+        stages.append(here)
+    for k, z in stages[-1]:
+
+        @pl.when(net.inside(z))
+        def _():
+            second(k, z)
+
+    for stage in stages[-2:]:
+        for k, z in stage:
+
+            @pl.when(net.inside(z))
+            def _():
+                third(k, z)
+
+    for stage in stages:
+        for k, z in stage:
+
+            @pl.when(net.inside(z))
+            def _():
+                for kind in range(5):
+                    core(kind, k, z, net.oc).wait_recv()
+
+    def drain():
+        mine.wait()
+        for side, step in ((0, 1), (1, -1)):
+
+            @pl.when(net.inside(net.z + step))
+            def _():
+                to_z(1 + side, net.z, step, w_own).wait_send()
+
+        for step, side, k, z, onward in slots():
+            if step < net.zs - 2:
+
+                @pl.when(jnp.logical_and(net.inside(z), net.inside(net.z + onward)))
+                def _():
+                    to_z(k + 2, z, onward).wait_send()
+
+        for stage in stages:
+            for k, z in stage:
+
+                @pl.when(net.inside(z))
+                def _():
+                    to_x(k, z).wait_send()
+                    to_y(k, z).wait_send()
+                    diag_to(k, z, 0).wait_send()
+                    diag_to(k, z, 1).wait_send()
+                    for kind in range(5):
+                        core(kind, k, z, net.c).wait_send()
+
+    drain()
+
+
+def project_kernel(
+    dims, scale, head_width, tok_ref, w_own, cos_ref, sin_ref, qg_ref, kg_ref, q_ref, kv_ref,
+    wbuf, *sems
+):
+    net = Net(dims)
+    greet(net, (net.at(x=net.ox), net.at(y=net.oy), net.at(c=net.oc)))
+    gather_weights(net, w_own, wbuf, *sems)
+    rows, width = cos_ref.shape
+    depth = tok_ref.shape[1]
+    kv_width = kv_ref.shape[1] // 2
+    pair = 2 * head_width
+    r = lax.broadcasted_iota(jnp.int32, (width, width), 0) // head_width
+    c = lax.broadcasted_iota(jnp.int32, (width, width), 1) // head_width
+    averager = jnp.where(r == c, 1.0 / head_width, 0.0).astype(jnp.float32)
+    lane = lax.broadcasted_iota(jnp.int32, (rows, width), 1)
+    first = lane % (head_width // 2) < head_width // 4
+    low = lax.broadcasted_iota(jnp.int32, (rows, pair), 1) < head_width
+
+    def product(at):
+        w = wbuf[:, :, :, :, :, at : at + width].reshape(depth, width)
+        return jnp.dot(tok_ref[...], w, preferred_element_type=jnp.float32)
+
+    def turned(t, gain):
+        mean_sq = jnp.dot(
+            t * t, averager, precision=lax.Precision.HIGHEST, preferred_element_type=jnp.float32
+        )
+        t = t * lax.rsqrt(mean_sq + epsilon) * gain
+        quarter = head_width // 4
+        other = jnp.where(first, pltpu.roll(t, width - quarter, 1), pltpu.roll(t, quarter, 1))
+        return t * cos_ref[...] + other * sin_ref[...]
+
+    per = width // head_width
+    for j in range(kv_width // width):
+        k = turned(product(j * width), kg_ref[...])
+        v = product(kv_width + j * width)
+        for i in range(0, per, 2):
+            kp = k[:, i * head_width : i * head_width + pair]
+            vp = v[:, i * head_width : i * head_width + pair]
+            at = (j * per + i) * pair
+            kv_ref[:, at : at + pair] = jnp.where(low, kp, pltpu.roll(vp, head_width, 1)).astype(
+                kv_ref.dtype
+            )
+            kv_ref[:, at + pair : at + 2 * pair] = jnp.where(
+                low, pltpu.roll(kp, head_width, 1), vp
+            ).astype(kv_ref.dtype)
+    for j in range(q_ref.shape[0] // per):
+        q = turned(product(2 * kv_width + j * width), qg_ref[...])
+        q = q.astype(q_ref.dtype).astype(jnp.float32) * scale
+        for i in range(0, per, 2):
+            qp = q[:, i * head_width : i * head_width + pair]
+            q_ref[j * per + i] = jnp.where(low, qp, 0.0).astype(q_ref.dtype)
+            q_ref[j * per + i + 1] = jnp.where(low, pltpu.roll(qp, head_width, 1), 0.0).astype(
+                q_ref.dtype
+            )
+
+
+def gather_kv(net, own, buf, own_sem, zs_sem, zr_sem, xs, xr):
+    def block(z, x):
+        return buf.at[z, x]
+
+    def to_z(k, z, step, src=None):
+        dst = block(z, net.x)
+        return remote(
+            dst if src is None else src, dst, zs_sem.at[k], zr_sem.at[k], net.at(z=net.z + step)
+        )
+
+    def to_x(k, z, src=None):
+        dst = block(z, net.x)
+        return remote(dst if src is None else src, dst, xs.at[k], xr.at[k], net.at(x=net.ox))
+
+    def from_x(k, z):
+        b = block(z, net.ox)
+        return remote(b, b, xs.at[k], xr.at[k], net.at(x=net.ox))
+
+    mine = pltpu.make_async_copy(own, block(net.z, net.x), own_sem)
+    mine.start()
+    to_x(0, net.z, own).start()
+    for side, step in ((0, 1), (1, -1)):
+
+        @pl.when(net.inside(net.z + step))
+        def _():
+            to_z(1 + side, net.z, step, own).start()
+
+    slots = [
+        (s, 1 + 2 * s + side, net.z + sign * (s + 1), -sign)
+        for s in range(net.zs - 1)
+        for side, sign in ((0, -1), (1, 1))
+    ]
+    for s, k, z, onward in slots:
+
+        @pl.when(net.inside(z))
+        def _():
+            to_z(k, z, 0).wait_recv()
+            if s < net.zs - 2:
+
+                @pl.when(net.inside(net.z + onward))
+                def _():
+                    to_z(k + 2, z, onward).start()
+
+            to_x(k, z).start()
+
+    from_x(0, net.z).wait_recv()
+    to_x(0, net.z, own).wait_send()
+    mine.wait()
+    for side, step in ((0, 1), (1, -1)):
+
+        @pl.when(net.inside(net.z + step))
+        def _():
+            to_z(1 + side, net.z, step, own).wait_send()
+
+    for s, k, z, onward in slots:
+
+        @pl.when(net.inside(z))
+        def _():
+            from_x(k, z).wait_recv()
+            to_x(k, z).wait_send()
+            if s < net.zs - 2:
+
+                @pl.when(net.inside(net.z + onward))
+                def _():
+                    to_z(k + 2, z, onward).wait_send()
+
+
+def softmax_rows(q, keys, split):
+    s = lax.dot_general(q, keys, (((1,), (1,)), ((), ())), preferred_element_type=jnp.float32)
+    p = jnp.exp(s - jnp.max(s, axis=-1, keepdims=True))
+    total = jnp.sum(p, axis=-1, keepdims=True)
+    o = jnp.dot(p.astype(jnp.bfloat16), keys, preferred_element_type=jnp.float32)
+    return o / total
+
+
+def attend_kernel(dims, group, q_ref, kv_ref, out_ref, buf, *sems):
+    net = Net(dims)
+    greet(net, (net.at(x=net.ox),))
+    gather_kv(net, kv_ref, buf, *sems)
+    heads, rows, pair = q_ref.shape
+    total = buf.shape[0] * buf.shape[1] * buf.shape[2]
+    block = 128 if rows % 128 == 0 else rows
+    low = lax.broadcasted_iota(jnp.int32, (block, pair), 1) < pair // 2
+
+    def step(j, carry):
+        g = j // (group // 2)
+        keys = buf[:, :, :, pl.ds(pl.multiple_of(g * pair, pair), pair)].reshape(total, pair)
+        for i in range(rows // block):
+            at = pl.ds(i * block, block)
+            a = softmax_rows(q_ref[2 * j, at, :], keys, pair // 2)
+            b = softmax_rows(q_ref[2 * j + 1, at, :], keys, pair // 2)
+            out_ref[at, pl.ds(pl.multiple_of(j * pair, pair), pair)] = jnp.where(
+                low, pltpu.roll(a, pair // 2, 1), b
+            ).astype(out_ref.dtype)
+        return carry
+
+    lax.fori_loop(0, heads // 2, step, 0)
+
+
+def vmem():
+    return pl.BlockSpec(memory_space=pltpu.VMEM)
+
+
+def fast(dims, tokens, q_weight, k_weight, v_weight, out_weight, q_gain, k_gain):
+    zs, xs, ys = dims
+    rows_in = tokens[0]
+    tok_count, depth = rows_in.shape
+    head_width = q_gain.shape[0]
+    q_heads = out_weight.shape[0] // head_width
+    kv_width = k_weight.shape[1]
+    group = q_heads // (kv_width // head_width)
+    offset = lax.axis_index("sp") * tok_count
+    width = 4 * head_width
+    cos, sin = tables(tok_count, head_width, offset, width)
+    own = jnp.concatenate([k_weight, v_weight, q_weight], axis=1)
+    pair = 2 * head_width
+    dma = pltpu.SemaphoreType.DMA
+    n = 1 + 2 * (zs - 1)
+    out_full = lax.all_gather(out_weight, ("sp", "dp"), axis=1, tiled=True)
+    q, kv = pl.pallas_call(
+        functools.partial(project_kernel, dims, head_width ** (-0.5), head_width),
+        out_shape=(
+            jax.ShapeDtypeStruct((q_heads, tok_count, pair), jnp.bfloat16),
+            jax.ShapeDtypeStruct((tok_count, 2 * kv_width), jnp.bfloat16),
+        ),
+        in_specs=[vmem()] * 6,
+        out_specs=(vmem(), vmem()),
+        scratch_shapes=[
+            pltpu.VMEM((zs, xs, ys, CORES) + own.shape, jnp.bfloat16),
+            dma,
+            dma((n,)), dma((n,)), dma((n,)), dma((n,)), dma((n,)), dma((n,)),
+            dma((2, n)), dma((2, n)), dma((5, n)), dma((5, n)),
+        ],
+        compiler_params=pltpu.CompilerParams(
+            collective_id=0, has_side_effects=True, vmem_limit_bytes=VMEM_BYTES
+        ),
+        cost_estimate=pl.CostEstimate(
+            flops=60_000_000_000, bytes_accessed=10_000_000, transcendentals=0
+        ),
+    )(
+        rows_in, own, cos, sin,
+        jnp.tile(q_gain, width // head_width)[None], jnp.tile(k_gain, width // head_width)[None],
+    )
+    attended = pl.pallas_call(
+        functools.partial(attend_kernel, dims, group),
+        out_shape=jax.ShapeDtypeStruct((tok_count, q_heads * head_width), jnp.bfloat16),
+        in_specs=[vmem()] * 2,
+        out_specs=vmem(),
+        scratch_shapes=[
+            pltpu.VMEM((zs, xs) + kv.shape, jnp.bfloat16),
+            dma,
+            dma((n,)), dma((n,)), dma((n,)), dma((n,)),
+        ],
+        compiler_params=pltpu.CompilerParams(
+            collective_id=1, has_side_effects=True, vmem_limit_bytes=VMEM_BYTES
+        ),
+        cost_estimate=pl.CostEstimate(
+            flops=60_000_000_000, bytes_accessed=10_000_000, transcendentals=20_000_000
+        ),
+    )(q, kv)
+    result = jnp.dot(attended, out_full, preferred_element_type=jnp.float32)
+    return result.astype(jnp.bfloat16)[None]
 
 
 def normalize(tensor, gain_vec):
@@ -66,7 +523,7 @@
     return lax.map(attend_block, blocks).reshape(row_count, head_width)
 
 
-def per_device(tokens, q_weight, k_weight, v_weight, out_weight, q_gain, k_gain):
+def plain(tokens, q_weight, k_weight, v_weight, out_weight, q_gain, k_gain):
     rows_in = tokens[0]
     tok_count = rows_in.shape[0]
     head_width = q_gain.shape[0]
@@ -131,8 +588,12 @@
 
 
 def solution(mesh):
+    sp, dp = mesh.shape["sp"], mesh.shape["dp"]
+    across = dp // CORES
+    exchange = dp == 2 * CORES and sp % across == 0 and sp // across > 1
+    body = functools.partial(fast, (sp // across, across, across)) if exchange else plain
     return jax.shard_map(
-        per_device,
+        body,
         mesh=mesh,
         in_specs=(
             P("dp", "sp", None),

time: 336 us -> 157 us (0.47)
  waiting for transfers between devices: 210 us -> 0.7 us
  Pallas kernels: 0 us -> 133 us
  matrix products: 55.7 us -> 5.4 us
  local copies, waits for them, and re-layouts: 23 us -> 3.23 us
  starting transfers between devices: 16.8 us -> 0.04 us
  other arithmetic: 15.1 us -> 1 us
    all_gather x4 -> x1, waiting for transfers between devices: 145 us -> 0.02 us  [fast(): out_full = lax.all_gather(out_weight, ('sp', 'dp'), axis=1, tiled=True)]
    pallas_call x0 -> x2, Pallas kernels: none -> 133 us  [the longest x1 85 us: fast(): pl.pallas_call(functools.partial(attend_kernel, dims, group), out_shape=j...]
    all_to_all x4 -> x0, waiting for transfers between devices: 62.6 us -> none  [the longest x1 21.5 us: per_device(): lax.all_to_all(values_wide, 'sp', split_axis=1, concat_axis=0, tiled=True)]
    dot_general x28 -> x1, matrix products: 55.7 us -> 5.4 us  [fast(): result = jnp.dot(attended, out_full, preferred_element_type=jnp.float32)]
    all_to_all x4 -> x0, starting transfers between devices: 16.7 us -> none  [the longest x1 4.41 us: per_device(): lax.all_to_all(queries.reshape(tok_count, q_width), 'sp', split_axis=1, c...]
    reduce_sum x12 -> x0, other arithmetic: 13.9 us -> none  [attend_block(): jnp.sum(weights, axis=-1, keepdims=True)]
    dot_general x2 -> x0, local copies, waits for them, and re-layouts: 8 us -> none  [per_device(): jnp.dot(rows_in, rows_part, preferred_element_type=jnp.float32)]
    slice x3 -> x0, local copies, waits for them, and re-layouts: 7.42 us -> none  [the longest x1 2.85 us: per_device(): q_local[:, low_col:low_col + head_width]]
  transfers between devices with their start and end apart: 8 -> 1, of which waited for: 6 -> 0; matrix products, arithmetic and copies ran while one was open for 26% -> 3% of each run, Pallas kernels for 0% -> 85%
where the time goes in v1:
time: 157 us
  Pallas kernels  133 us (85%)
  between operations  13.5 us (9%)
  matrix products  5.4 us (3%)
  local copies, waits for them, and re-layouts  3.23 us (2%)
    pallas_call x1, Pallas kernels, fast(): pl.pallas_call(functools.partial(attend_kernel, dims, group), out_shape=j...  85 us
    pallas_call x1, Pallas kernels, fast(): pl.pallas_call(functools.partial(project_kernel, dims, head_width ** (-0....  47.7 us
    dot_general x1, matrix products, fast(): result = jnp.dot(attended, out_full, preferred_element_type=jnp.float32)  5.4 us
  transfers between devices with their start and end apart: 1, of which 0 were waited for; matrix products, arithmetic and copies ran while one was open for 3% of the time, Pallas kernels for 85%

profile of v1, /device:TPU:0, one launch (start us, length us, event | category | flops | bytes accessed | tf_op | source)
XLA Modules:
  0.0 156.5 jit_solution(3504352499601162890)
XLA Ops:
  6.5 0.0 copy-start.3
  6.5 0.0 copy-start.4
  6.5 0.0 copy-start.1
  6.5 0.0 copy-start
  6.5 0.0 copy-start.2
  6.5 0.0 all-gather.2.cloned.1.call-start
  6.6 0.7 all-gather.2.cloned.1.call-update
  7.3 0.3 fusion.1
  7.6 0.9 copy.9.sin_ref
  8.6 0.9 copy.8.cos_ref
  9.5 0.0 copy-done.3
  9.5 0.7 broadcast_in_dim_tile.6.qg_ref
  10.2 0.0 copy-done.4
  10.2 0.7 broadcast_in_dim_tile.7.kg_ref
  10.8 0.0 copy-done.1
  10.8 0.0 copy-done
  10.8 0.0 copy-done.2
  10.9 0.7 pad_maximum_fusion.w_own
  11.6 47.7 %shard_map.73 = (bf16[16,384,128]{2,1,0:T(8,128)(2,1)}, bf16[384,512]{1,0:T(8,128)(2,1)}) custom-call(bf16[384,2048]{1,0:T(8,128)(2,1)} %bitcast.9, bf16[64,1536]{1,0:T(8,128)(2,1)} %pad_maximum_fusion.w_own, f32[384,256]{1,0:T(8,128)} %copy.8.cos_ref, f32[384,256]{1,0:T(8,128)} %copy.9.sin_ref, f32[1,256]{1,0:T(1,128)} %broadcast_in_dim_tile.6.qg_ref, ...), custom_call_target="tpu_custom_call" | custom-call | flops 60000002048 | bytes 10000000 | tf_op jit(solution)/shard_map/pallas_call | solution.py:427
  59.3 85.0 %shard_map.74 = bf16[384,1024]{1,0:T(8,128)(2,1)} custom-call(bf16[16,384,128]{2,1,0:T(8,128)(2,1)} %get-tuple-element.7.q_ref, bf16[384,512]{1,0:T(8,128)(2,1)} %get-tuple-element.8.kv_ref), custom_call_target="tpu_custom_call" | custom-call | flops 60000002048 | bytes 10000000 | tf_op jit(solution)/shard_map/pallas_call | solution.py:451
  144.3 0.0 all-gather.2.cloned.1.call-done
  144.3 5.4 %fusion = bf16[1,384,2048]{2,1,0:T(8,128)(2,1)} fusion(bf16[384,1024]{1,0:T(8,128)(2,1)} %shard_map.74, bf16[1024,2048]{0,1:T(8,128)(2,1)} %all-gather.2.cloned.1.call-done), kind=kOutput, calls=%fused_computation.1 | convolution fusion | flops 1611399168 | bytes 6553600 | tf_op jit(solution)/shard_map/dot_general | solution.py:468
  (8 shorter events, 0.1 us)
Async XLA Ops:
  6.5 3.0 %copy-start.3 = (f32[64]{0:T(128)S(1)}, f32[64]{0:T(128)}, u32[]{:S(2)}) copy-start(f32[64]{0:T(128)} %param.12) | copy-start | bytes 772
  6.5 3.6 %copy-start.4 = (f32[64]{0:T(128)S(1)}, f32[64]{0:T(128)}, u32[]{:S(2)}) copy-start(f32[64]{0:T(128)} %param.13) | copy-start | bytes 772
  6.5 4.3 %copy-start.1 = (bf16[64,256]{1,0:T(8,128)(2,1)S(1)}, bf16[64,256]{1,0:T(8,128)(2,1)}, u32[]{:S(2)}) copy-start(bf16[64,256]{1,0:T(8,128)(2,1)} %param.10) | copy-start | bytes 98308
  6.5 4.3 %copy-start = (bf16[64,1024]{1,0:T(8,128)(2,1)S(1)}, bf16[64,1024]{1,0:T(8,128)(2,1)}, u32[]{:S(2)}) copy-start(bf16[64,1024]{1,0:T(8,128)(2,1)} %param.8) | copy-start | bytes 393220
  6.5 4.3 %copy-start.2 = (bf16[64,256]{1,0:T(8,128)(2,1)S(1)}, bf16[64,256]{1,0:T(8,128)(2,1)}, u32[]{:S(2)}) copy-start(bf16[64,256]{1,0:T(8,128)(2,1)} %param.9) | copy-start | bytes 98308
  6.5 137.7 %all-gather.2.cloned.1.call-start = ((), (), s32[]{:S(2)}) async-start(), calls=%async_computation | async-start | bytes 4325376 | tf_op jit(solution)/shard_map/all_gather | solution.py:426
Sparse Core Ops, SparseCore 0:
  10.2 76.1 all-gather.1

commit v2 on v1

--- a/solution.py
+++ b/solution.py
@@ -249,13 +249,92 @@
     drain()
 
 
-def project_kernel(
-    dims, scale, head_width, tok_ref, w_own, cos_ref, sin_ref, qg_ref, kg_ref, q_ref, kv_ref,
-    wbuf, *sems
+def exchange(net, own, buf, own_sem, zs_sem, zr_sem, xs, xr):
+    last = 2 * (net.zs - 1)
+
+    def block(z, x):
+        return buf.at[z, x]
+
+    def to_z(k, z, step, src=None):
+        dst = block(z, net.x)
+        return remote(
+            dst if src is None else src, dst, zs_sem.at[k], zr_sem.at[k], net.at(z=net.z + step)
+        )
+
+    def to_x(k, z, src=None):
+        dst = block(z, net.x)
+        return remote(dst if src is None else src, dst, xs.at[k], xr.at[k], net.at(x=net.ox))
+
+    def from_x(k, z):
+        b = block(z, net.ox)
+        return remote(b, b, xs.at[k], xr.at[k], net.at(x=net.ox))
+
+    def owner(k):
+        return net.z + jnp.where(k % 2 == 1, -1, 1) * ((k + 1) // 2)
+
+    def goes_on(k):
+        return jnp.logical_and(k + 2 <= last, net.inside(net.z + jnp.where(k % 2 == 1, 1, -1)))
+
+    mine = pltpu.make_async_copy(own, block(net.z, net.x), own_sem)
+
+    def start():
+        mine.start()
+        for side, step in ((0, 1), (1, -1)):
+
+            @pl.when(net.inside(net.z + step))
+            def _():
+                to_z(1 + side, net.z, step, own).start()
+
+        to_x(0, net.z, own).start()
+
+    def pass_on(k):
+        z = owner(k)
+
+        @pl.when(jnp.logical_and(k <= last, net.inside(z)))
+        def _():
+            to_z(k, z, 0).wait_recv()
+
+            @pl.when(goes_on(k))
+            def _():
+                to_z(k + 2, z, jnp.where(k % 2 == 1, 1, -1)).start()
+
+            to_x(k, z).start()
+
+    def drain():
+        for side, step in ((0, 1), (1, -1)):
+
+            @pl.when(net.inside(net.z + step))
+            def _():
+                to_z(1 + side, net.z, step, own).wait_send()
+
+        to_x(0, net.z, own).wait_send()
+
+        def one(k, carry):
+            z = owner(k)
+
+            @pl.when(net.inside(z))
+            def _():
+                to_x(k, z).wait_send()
+
+                @pl.when(goes_on(k))
+                def _():
+                    to_z(k + 2, z, jnp.where(k % 2 == 1, 1, -1)).wait_send()
+
+            return carry
+
+        lax.fori_loop(1, last + 1, one, 0)
+
+    return mine, owner, from_x, start, pass_on, drain
+
+
+def layer_kernel(
+    dims, group, scale, head_width, tok_ref, w_own, cos_ref, sin_ref, qg_ref, kg_ref, out_ref,
+    wbuf, q_ref, kv_ref, buf, acc_ref, max_ref, sum_ref, *sems
 ):
     net = Net(dims)
     greet(net, (net.at(x=net.ox), net.at(y=net.oy), net.at(c=net.oc)))
-    gather_weights(net, w_own, wbuf, *sems)
+    gather_weights(net, w_own, wbuf, *sems[:11])
+    mine, owner, from_x, start, pass_on, drain = exchange(net, kv_ref, buf, *sems[11:])
     rows, width = cos_ref.shape
     depth = tok_ref.shape[1]
     kv_width = kv_ref.shape[1] // 2
@@ -294,7 +373,12 @@
             kv_ref[:, at + pair : at + 2 * pair] = jnp.where(
                 low, pltpu.roll(kp, head_width, 1), vp
             ).astype(kv_ref.dtype)
+    max_ref[...] = jnp.full_like(max_ref, -jnp.inf)
+    sum_ref[...] = jnp.zeros_like(sum_ref)
+    acc_ref[...] = jnp.zeros_like(acc_ref)
     for j in range(q_ref.shape[0] // per):
+        if j == 1:
+            start()
         q = turned(product(2 * kv_width + j * width), qg_ref[...])
         q = q.astype(q_ref.dtype).astype(jnp.float32) * scale
         for i in range(0, per, 2):
@@ -304,104 +388,70 @@
                 q_ref.dtype
             )
 
-
-def gather_kv(net, own, buf, own_sem, zs_sem, zr_sem, xs, xr):
-    def block(z, x):
-        return buf.at[z, x]
-
-    def to_z(k, z, step, src=None):
-        dst = block(z, net.x)
-        return remote(
-            dst if src is None else src, dst, zs_sem.at[k], zr_sem.at[k], net.at(z=net.z + step)
-        )
-
-    def to_x(k, z, src=None):
-        dst = block(z, net.x)
-        return remote(dst if src is None else src, dst, xs.at[k], xr.at[k], net.at(x=net.ox))
-
-    def from_x(k, z):
-        b = block(z, net.ox)
-        return remote(b, b, xs.at[k], xr.at[k], net.at(x=net.ox))
-
-    mine = pltpu.make_async_copy(own, block(net.z, net.x), own_sem)
-    mine.start()
-    to_x(0, net.z, own).start()
-    for side, step in ((0, 1), (1, -1)):
-
-        @pl.when(net.inside(net.z + step))
+    block = 128 if rows % 128 == 0 else rows
+    blocks = [pl.ds(i * block, block) for i in range(rows // block)]
+    keys_now = buf.shape[1] * rows
+    pairs = q_ref.shape[0] // 2
+
+    def update(h, at, keys):
+        s = lax.dot_general(
+            q_ref[h, at, :], keys, (((1,), (1,)), ((), ())), preferred_element_type=jnp.float32
+        )
+        old = max_ref[h, at, :]
+        top = jnp.maximum(old, jnp.max(s, axis=-1, keepdims=True))
+        p = jnp.exp(s - jnp.concatenate([top] * (keys_now // pair), axis=1))
+        fade = jnp.exp(old - top)
+        max_ref[h, at, :] = top
+        sum_ref[h, at, :] = sum_ref[h, at, :] * fade + jnp.sum(p, axis=-1, keepdims=True)
+        acc_ref[h, at, :] = acc_ref[h, at, :] * fade + jnp.dot(
+            p.astype(keys.dtype), keys, preferred_element_type=jnp.float32
+        )
+
+    def attend(z):
+        def step(j, carry):
+            g = j // (group // 2)
+            keys = buf[z, :, :, pl.ds(pl.multiple_of(g * pair, pair), pair)]
+            keys = keys.reshape(keys_now, pair)
+            for at in blocks:
+                update(2 * j, at, keys)
+                update(2 * j + 1, at, keys)
+            return carry
+
+        lax.fori_loop(0, pairs, step, 0)
+
+    pass_on(1)
+    pass_on(2)
+    mine.wait()
+
+    def arrival(k, carry):
+        @pl.when(k % 2 == 1)
         def _():
-            to_z(1 + side, net.z, step, own).start()
-
-    slots = [
-        (s, 1 + 2 * s + side, net.z + sign * (s + 1), -sign)
-        for s in range(net.zs - 1)
-        for side, sign in ((0, -1), (1, 1))
-    ]
-    for s, k, z, onward in slots:
-
-        @pl.when(net.inside(z))
-        def _():
-            to_z(k, z, 0).wait_recv()
-            if s < net.zs - 2:
-
-                @pl.when(net.inside(net.z + onward))
-                def _():
-                    to_z(k + 2, z, onward).start()
-
-            to_x(k, z).start()
-
-    from_x(0, net.z).wait_recv()
-    to_x(0, net.z, own).wait_send()
-    mine.wait()
-    for side, step in ((0, 1), (1, -1)):
-
-        @pl.when(net.inside(net.z + step))
-        def _():
-            to_z(1 + side, net.z, step, own).wait_send()
-
-    for s, k, z, onward in slots:
+            pass_on(k + 2)
+            pass_on(k + 3)
+
+        z = owner(k)
 
         @pl.when(net.inside(z))
         def _():
             from_x(k, z).wait_recv()
-            to_x(k, z).wait_send()
-            if s < net.zs - 2:
-
-                @pl.when(net.inside(net.z + onward))
-                def _():
-                    to_z(k + 2, z, onward).wait_send()
-
-
-def softmax_rows(q, keys, split):
-    s = lax.dot_general(q, keys, (((1,), (1,)), ((), ())), preferred_element_type=jnp.float32)
-    p = jnp.exp(s - jnp.max(s, axis=-1, keepdims=True))
-    total = jnp.sum(p, axis=-1, keepdims=True)
-    o = jnp.dot(p.astype(jnp.bfloat16), keys, preferred_element_type=jnp.float32)
-    return o / total
-
-
-def attend_kernel(dims, group, q_ref, kv_ref, out_ref, buf, *sems):
-    net = Net(dims)
-    greet(net, (net.at(x=net.ox),))
-    gather_kv(net, kv_ref, buf, *sems)
-    heads, rows, pair = q_ref.shape
-    total = buf.shape[0] * buf.shape[1] * buf.shape[2]
-    block = 128 if rows % 128 == 0 else rows
-    low = lax.broadcasted_iota(jnp.int32, (block, pair), 1) < pair // 2
-
-    def step(j, carry):
-        g = j // (group // 2)
-        keys = buf[:, :, :, pl.ds(pl.multiple_of(g * pair, pair), pair)].reshape(total, pair)
-        for i in range(rows // block):
-            at = pl.ds(i * block, block)
-            a = softmax_rows(q_ref[2 * j, at, :], keys, pair // 2)
-            b = softmax_rows(q_ref[2 * j + 1, at, :], keys, pair // 2)
+            attend(z)
+
+        return carry
+
+    lax.fori_loop(0, 2 * (net.zs - 1) + 1, arrival, 0)
+    low_block = lax.broadcasted_iota(jnp.int32, (block, pair), 1) < head_width
+
+    def finish(j, carry):
+        for at in blocks:
+            a = acc_ref[2 * j, at, :] / sum_ref[2 * j, at, :]
+            b = acc_ref[2 * j + 1, at, :] / sum_ref[2 * j + 1, at, :]
             out_ref[at, pl.ds(pl.multiple_of(j * pair, pair), pair)] = jnp.where(
-                low, pltpu.roll(a, pair // 2, 1), b
+                low_block, pltpu.roll(a, head_width, 1), b
             ).astype(out_ref.dtype)
         return carry
 
-    lax.fori_loop(0, heads // 2, step, 0)
+    lax.fori_loop(0, pairs, finish, 0)
+    drain()
 
 
 def vmem():
@@ -424,47 +474,35 @@
     dma = pltpu.SemaphoreType.DMA
     n = 1 + 2 * (zs - 1)
     out_full = lax.all_gather(out_weight, ("sp", "dp"), axis=1, tiled=True)
-    q, kv = pl.pallas_call(
-        functools.partial(project_kernel, dims, head_width ** (-0.5), head_width),
-        out_shape=(
-            jax.ShapeDtypeStruct((q_heads, tok_count, pair), jnp.bfloat16),
-            jax.ShapeDtypeStruct((tok_count, 2 * kv_width), jnp.bfloat16),
-        ),
+    attended = pl.pallas_call(
+        functools.partial(layer_kernel, dims, group, head_width ** (-0.5), head_width),
+        out_shape=jax.ShapeDtypeStruct((tok_count, q_heads * head_width), jnp.bfloat16),
         in_specs=[vmem()] * 6,
-        out_specs=(vmem(), vmem()),
+        out_specs=vmem(),
         scratch_shapes=[
             pltpu.VMEM((zs, xs, ys, CORES) + own.shape, jnp.bfloat16),
+            pltpu.VMEM((q_heads, tok_count, pair), jnp.bfloat16),
+            pltpu.VMEM((tok_count, 2 * kv_width), jnp.bfloat16),
+            pltpu.VMEM((zs, xs, tok_count, 2 * kv_width), jnp.bfloat16),
+            pltpu.VMEM((q_heads, tok_count, pair), jnp.float32),
+            pltpu.VMEM((q_heads, tok_count, pair), jnp.float32),
+            pltpu.VMEM((q_heads, tok_count, pair), jnp.float32),
             dma,
             dma((n,)), dma((n,)), dma((n,)), dma((n,)), dma((n,)), dma((n,)),
             dma((2, n)), dma((2, n)), dma((5, n)), dma((5, n)),
+            dma,
+            dma((n,)), dma((n,)), dma((n,)), dma((n,)),
         ],
         compiler_params=pltpu.CompilerParams(
             collective_id=0, has_side_effects=True, vmem_limit_bytes=VMEM_BYTES
         ),
         cost_estimate=pl.CostEstimate(
-            flops=60_000_000_000, bytes_accessed=10_000_000, transcendentals=0
+            flops=100_000_000_000, bytes_accessed=10_000_000, transcendentals=20_000_000
         ),
     )(
         rows_in, own, cos, sin,
         jnp.tile(q_gain, width // head_width)[None], jnp.tile(k_gain, width // head_width)[None],
     )
-    attended = pl.pallas_call(
-        functools.partial(attend_kernel, dims, group),
-        out_shape=jax.ShapeDtypeStruct((tok_count, q_heads * head_width), jnp.bfloat16),
-        in_specs=[vmem()] * 2,
-        out_specs=vmem(),
-        scratch_shapes=[
-            pltpu.VMEM((zs, xs) + kv.shape, jnp.bfloat16),
-            dma,
-            dma((n,)), dma((n,)), dma((n,)), dma((n,)),
-        ],
-        compiler_params=pltpu.CompilerParams(
-            collective_id=1, has_side_effects=True, vmem_limit_bytes=VMEM_BYTES
-        ),
-        cost_estimate=pl.CostEstimate(
-            flops=60_000_000_000, bytes_accessed=10_000_000, transcendentals=20_000_000
-        ),
-    )(q, kv)
     result = jnp.dot(attended, out_full, preferred_element_type=jnp.float32)
     return result.astype(jnp.bfloat16)[None]
 

time: 157 us -> 157 us (level)
  Pallas kernels: 133 us -> 131 us
    pallas_call x2 -> x1, Pallas kernels: 133 us -> 131 us  [fast(): pl.pallas_call(functools.partial(layer_kernel, dims, group, head_width **...]
  transfers between devices with their start and end apart: 1 -> 1, of which waited for: 0 -> 0; matrix products, arithmetic and copies ran while one was open for 3% -> 4% of each run, Pallas kernels for 85% -> 83%
where the time goes in v2:
time: 157 us
  Pallas kernels  131 us (83%)
  between operations  13.4 us (9%)
  matrix products  5.41 us (3%)
  local copies, waits for them, and re-layouts  4.54 us (3%)
  other arithmetic  1.92 us (1%)
    pallas_call x1, Pallas kernels, fast(): pl.pallas_call(functools.partial(layer_kernel, dims, group, head_width **...  131 us
    dot_general x1, matrix products, fast(): result = jnp.dot(attended, out_full, preferred_element_type=jnp.float32)  5.41 us
  transfers between devices with their start and end apart: 1, of which 0 were waited for; matrix products, arithmetic and copies ran while one was open for 4% of the time, Pallas kernels for 83%

profile of v2, /device:TPU:0, one launch (start us, length us, event | category | flops | bytes accessed | tf_op | source)
XLA Modules:
  0.0 157.1 jit_solution(12099841963038585882)
XLA Ops:
  6.5 0.0 all-gather.2.cloned.1.call-start
  6.5 0.7 all-gather.2.cloned.1.call-update
  7.3 0.7 tile.16
  7.9 0.7 broadcast_in_dim_tile.6.qg_ref
  8.6 0.7 tile.17
  9.3 0.7 broadcast_in_dim_tile.7.kg_ref
  10.0 0.3 fusion.1
  10.3 0.9 copy.8.cos_ref
  11.2 0.9 copy.9.sin_ref
  12.1 1.6 %pad_maximum_fusion.w_own = bf16[64,1536]{1,0:T(8,128)(2,1)} fusion(bf16[64,1024]{1,0:T(8,128)(2,1)} %param.8, bf16[64,256]{1,0:T(8,128)(2,1)} %param.10, bf16[64,256]{1,0:T(8,128)(2,1)} %param.9), kind=kLoop, calls=%fused_computation.2 | loop fusion | flops 589824 | bytes 393216 | tf_op jit(solution)/shard_map/concatenate | solution.py:472
  13.8 131.0 %shard_map.73 = bf16[384,1024]{1,0:T(8,128)(2,1)} custom-call(bf16[384,2048]{1,0:T(8,128)(2,1)} %bitcast.9, bf16[64,1536]{1,0:T(8,128)(2,1)} %pad_maximum_fusion.w_own, f32[384,256]{1,0:T(8,128)} %copy.8.cos_ref, f32[384,256]{1,0:T(8,128)} %copy.9.sin_ref, f32[1,256]{1,0:T(1,128)} %broadcast_in_dim_tile.6.qg_ref, f32[1,256]{1,0:T(1,128)} %broadcast_in_dim_tile.7.kg_ref), custom_call_target="tpu_custom_call" | custom-call | flops 99999997952 | bytes 10000000 | tf_op jit(solution)/shard_map/pallas_call | solution.py:477
  144.8 0.0 all-gather.2.cloned.1.call-done
  144.8 5.4 %fusion = bf16[1,384,2048]{2,1,0:T(8,128)(2,1)} fusion(bf16[384,1024]{1,0:T(8,128)(2,1)} %shard_map.73, bf16[1024,2048]{0,1:T(8,128)(2,1)} %all-gather.2.cloned.1.call-done), kind=kOutput, calls=%fused_computation.1 | convolution fusion | flops 1611399168 | bytes 6553600 | tf_op jit(solution)/shard_map/dot_general | solution.py:506
  (6 shorter events, 0.1 us)
Async XLA Ops:
  6.5 138.3 %all-gather.2.cloned.1.call-start = ((), (), s32[]{:S(2)}) async-start(), calls=%async_computation | async-start | bytes 4325376 | tf_op jit(solution)/shard_map/all_gather | solution.py:476
Sparse Core Ops, SparseCore 0:
  10.2 74.2 all-gather.1

commit v3 on v2

--- a/solution.py
+++ b/solution.py
@@ -328,7 +328,7 @@
 
 
 def layer_kernel(
-    dims, group, scale, head_width, tok_ref, w_own, cos_ref, sin_ref, qg_ref, kg_ref, out_ref,
+    dims, group, scale, head_width, tok_ref, w_own, cos_ref, sin_ref, gain_ref, out_ref,
     wbuf, q_ref, kv_ref, buf, acc_ref, max_ref, sum_ref, *sems
 ):
     net = Net(dims)
@@ -361,7 +361,7 @@
 
     per = width // head_width
     for j in range(kv_width // width):
-        k = turned(product(j * width), kg_ref[...])
+        k = turned(product(j * width), gain_ref[1:2, :])
         v = product(kv_width + j * width)
         for i in range(0, per, 2):
             kp = k[:, i * head_width : i * head_width + pair]
@@ -379,7 +379,7 @@
     for j in range(q_ref.shape[0] // per):
         if j == 1:
             start()
-        q = turned(product(2 * kv_width + j * width), qg_ref[...])
+        q = turned(product(2 * kv_width + j * width), gain_ref[0:1, :])
         q = q.astype(q_ref.dtype).astype(jnp.float32) * scale
         for i in range(0, per, 2):
             qp = q[:, i * head_width : i * head_width + pair]
@@ -393,28 +393,31 @@
     keys_now = buf.shape[1] * rows
     pairs = q_ref.shape[0] // 2
 
-    def update(h, at, keys):
+    def update(h, keys, old, total, acc):
         s = lax.dot_general(
-            q_ref[h, at, :], keys, (((1,), (1,)), ((), ())), preferred_element_type=jnp.float32
-        )
-        old = max_ref[h, at, :]
+            q_ref[h], keys, (((1,), (1,)), ((), ())), preferred_element_type=jnp.float32
+        )
         top = jnp.maximum(old, jnp.max(s, axis=-1, keepdims=True))
         p = jnp.exp(s - jnp.concatenate([top] * (keys_now // pair), axis=1))
         fade = jnp.exp(old - top)
-        max_ref[h, at, :] = top
-        sum_ref[h, at, :] = sum_ref[h, at, :] * fade + jnp.sum(p, axis=-1, keepdims=True)
-        acc_ref[h, at, :] = acc_ref[h, at, :] * fade + jnp.dot(
+        total = total * fade + jnp.sum(p, axis=-1, keepdims=True)
+        acc = acc * fade + jnp.dot(
             p.astype(keys.dtype), keys, preferred_element_type=jnp.float32
         )
+        return top, total, acc
 
     def attend(z):
         def step(j, carry):
             g = j // (group // 2)
             keys = buf[z, :, :, pl.ds(pl.multiple_of(g * pair, pair), pair)]
             keys = keys.reshape(keys_now, pair)
-            for at in blocks:
-                update(2 * j, at, keys)
-                update(2 * j + 1, at, keys)
+            two = (2 * j, 2 * j + 1)
+            state = [(max_ref[h], sum_ref[h], acc_ref[h]) for h in two]
+            state = [update(h, keys, *held) for h, held in zip(two, state)]
+            for h, (top, total, acc) in zip(two, state):
+                max_ref[h] = top
+                sum_ref[h] = total
+                acc_ref[h] = acc
             return carry
 
         lax.fori_loop(0, pairs, step, 0)
@@ -477,7 +480,7 @@
     attended = pl.pallas_call(
         functools.partial(layer_kernel, dims, group, head_width ** (-0.5), head_width),
         out_shape=jax.ShapeDtypeStruct((tok_count, q_heads * head_width), jnp.bfloat16),
-        in_specs=[vmem()] * 6,
+        in_specs=[vmem()] * 5,
         out_specs=vmem(),
         scratch_shapes=[
             pltpu.VMEM((zs, xs, ys, CORES) + own.shape, jnp.bfloat16),
@@ -501,7 +504,7 @@
         ),
     )(
         rows_in, own, cos, sin,
-        jnp.tile(q_gain, width // head_width)[None], jnp.tile(k_gain, width // head_width)[None],
+        jnp.tile(jnp.stack([q_gain, k_gain]), (1, width // head_width)),
     )
     result = jnp.dot(attended, out_full, preferred_element_type=jnp.float32)
     return result.astype(jnp.bfloat16)[None]

time: 157 us -> 135 us (0.86)
  Pallas kernels: 131 us -> 110 us
  local copies, waits for them, and re-layouts: 4.54 us -> 2.56 us
    pallas_call x1, Pallas kernels: 131 us -> 110 us  [fast(): pl.pallas_call(functools.partial(layer_kernel, dims, group, head_width **...]
    another operation x4 -> x2, local copies, waits for them, and re-layouts: 2.66 us -> 0.68 us  [fast(): jnp.tile(jnp.stack([q_gain, k_gain]), (1, width // head_width))]
  transfers between devices with their start and end apart: 1 -> 1, of which waited for: 0 -> 0; matrix products, arithmetic and copies ran while one was open for 4% -> 4% of each run, Pallas kernels for 83% -> 82%
where the time goes in v3:
time: 135 us; the launch traced here: 134 us
  Pallas kernels  110 us (81%)
  between operations  13.4 us (10%)
  matrix products  5.4 us (4%)
  other arithmetic  2.6 us (2%)
  local copies, waits for them, and re-layouts  2.56 us (2%)
    pallas_call x1, Pallas kernels, fast(): pl.pallas_call(functools.partial(layer_kernel, dims, group, head_width **...  110 us
    dot_general x1, matrix products, fast(): result = jnp.dot(attended, out_full, preferred_element_type=jnp.float32)  5.4 us
  transfers between devices with their start and end apart: 1, of which 0 were waited for; matrix products, arithmetic and copies ran while one was open for 4% of the time, Pallas kernels for 82%

profile of v3, /device:TPU:0, one launch (start us, length us, event | category | flops | bytes accessed | tf_op | source)
XLA Modules:
  0.0 134.4 jit_solution(1457024559381651107)
XLA Ops:
  6.5 0.0 all-gather.2.cloned.1.call-start
  6.5 0.7 all-gather.2.cloned.1.call-update
  7.3 0.7 pad_maximum_fusion.3
  8.0 0.7 tile.32.gain_ref
  8.7 0.3 fusion.1
  9.0 0.9 copy.8.cos_ref
  9.9 0.9 copy.9.sin_ref
  10.8 1.6 %pad_maximum_fusion.w_own = bf16[64,1536]{1,0:T(8,128)(2,1)} fusion(bf16[64,1024]{1,0:T(8,128)(2,1)} %param.8, bf16[64,256]{1,0:T(8,128)(2,1)} %param.10, bf16[64,256]{1,0:T(8,128)(2,1)} %param.9), kind=kLoop, calls=%fused_computation.2 | loop fusion | flops 589824 | bytes 393216 | tf_op jit(solution)/shard_map/concatenate | solution.py:475
  12.5 109.7 %shard_map.73 = bf16[384,1024]{1,0:T(8,128)(2,1)} custom-call(bf16[384,2048]{1,0:T(8,128)(2,1)} %bitcast.13, bf16[64,1536]{1,0:T(8,128)(2,1)} %pad_maximum_fusion.w_own, f32[384,256]{1,0:T(8,128)} %copy.8.cos_ref, f32[384,256]{1,0:T(8,128)} %copy.9.sin_ref, f32[2,256]{1,0:T(2,128)} %tile.32.gain_ref), custom_call_target="tpu_custom_call" | custom-call | flops 99999997952 | bytes 10000000 | tf_op jit(solution)/shard_map/pallas_call | solution.py:480
  122.2 0.0 all-gather.2.cloned.1.call-done
  122.2 5.4 %fusion = bf16[1,384,2048]{2,1,0:T(8,128)(2,1)} fusion(bf16[384,1024]{1,0:T(8,128)(2,1)} %shard_map.73, bf16[1024,2048]{0,1:T(8,128)(2,1)} %all-gather.2.cloned.1.call-done), kind=kOutput, calls=%fused_computation.1 | convolution fusion | flops 1611399168 | bytes 6553600 | tf_op jit(solution)/shard_map/dot_general | solution.py:509
  (7 shorter events, 0.1 us)
Async XLA Ops:
  6.5 115.7 %all-gather.2.cloned.1.call-start = ((), (), s32[]{:S(2)}) async-start(), calls=%async_computation | async-start | bytes 4325376 | tf_op jit(solution)/shard_map/all_gather | solution.py:479
Sparse Core Ops, SparseCore 0:
  10.2 74.3 all-gather.1
